TPU v7x, 32 devices: a whole 2x2x4 slice. The times are simulated.
32 devices in a mesh: fs: 8 (over z, x), tp: 4 (over y, core).
Axes of the slice: x: 2, y: 2, z: 4, core: 2. Of those that a mesh axis runs over, the one named last changes fastest.
Arguments:
- saved_input: bfloat16 [49152, 2048], P(('fs', 'tp')), may hold values from -6 to 6
- value_cotangent: bfloat16 [49152, 1024], P(('fs', 'tp')), may hold values from -0.0546875 to 0.0546875
- decay_cotangent: bfloat16 [49152, 16], P(('fs', 'tp')), may hold values from -0.02734375 to 0.02734375
- value_master: float32 [2048, 1024], P('fs', 'tp'), may hold values from -6 to 6
- value_factor: bfloat16 [2048, 256], P('fs'), may hold values from -0.22097087 to 0.22097087
- value_mean: float32 [256, 1024], P('fs', 'tp'), may hold values from -0.625 to 0.625
- value_second: float32 [256, 1024], P('fs', 'tp'), may hold values from 0.0001 to 0.1
- decay_master: float32 [2048, 16], replicated, may hold values from -6 to 6
- decay_mean: float32 [2048, 16], replicated, may hold values from -0.625 to 0.625
- decay_second: float32 [2048, 16], replicated, may hold values from 0.001 to 0.01
Outputs:
- value_step: float32 [2048, 1024], P('fs', 'tp')
- value_new: float32 [2048, 1024], P('fs', 'tp')
- value_copy: bfloat16 [2048, 1024], P(None, 'tp')
- mean_new: float32 [256, 1024], P('fs', 'tp')
- second_new: float32 [256, 1024], P('fs', 'tp')
- decay_step: float32 [2048, 16], replicated
- decay_copy: bfloat16 [2048, 16], replicated
All inputs are finite; a program needn't handle non-finite values.
Results may differ from a plain program's by a relative error of at most 0.0004.
Values may be sent and summed in bfloat16 or wider, within the bound.
A program may use at most 64 MiB of HBM per device.

v0:
```python
import functools

import jax
import jax.numpy as jnp
from jax import lax
from jax.experimental import pallas as pl
from jax.experimental.pallas import tpu as pltpu
from jax.sharding import PartitionSpec as P

BETA_ONE = 0.9
BETA_TWO = 0.99
ADAM_EPS = 1e-08
RMS_EPS = 1e-06
LEARN_RATE = 0.05
LANES = 128
BF16 = jnp.bfloat16
F32 = jnp.float32


def flip(index, bits):
    result = index
    place = 1
    while place <= bits:
        if bits & place:
            result = result + place - 2 * place * ((index // place) % 2)
        place *= 2
    return result


def adam(moment_one, moment_two, gradient):
    mean_new = BETA_ONE * moment_one + (1.0 - BETA_ONE) * gradient
    second_new = BETA_TWO * moment_two + (1.0 - BETA_TWO) * gradient * gradient
    return mean_new, second_new, mean_new / (jnp.sqrt(second_new) + ADAM_EPS)


def dot(left, right):
    return jnp.dot(left, right, preferred_element_type=F32)


def kernel(
    fs_n, tp_n,
    x_hbm, c_hbm, dc_hbm, master_hbm, factor_hbm, mean_hbm, second_hbm,
    dmaster_hbm, dmean_hbm, dsecond_hbm,
    step_out, new_out, copy_out, mean_out, second_out, dstep_out, dcopy_out,
    x, c_in, dc, master, factor, mean, second, dmaster, dmean, dsecond,
    mapped, high, low, pa, pb, ra1, rb1, ra2, rb2, ra3, rb3, zed, rz,
    direction, squares, sq_tp, sq_fs, step_v, new_v, copy_v, mean_v, second_v,
    dpart, dr_tp, dmid, dr_fs, dgrad, dstep_v, dcopy_v,
    in_sem, out_sem,
    fz_s, fz_r, fx_s, fx_r, fc_s, fc_r,
    p1_s, p1_r, a2_s, a2_r, b2_s, b2_r, a3_s, a3_r, b3_s, b3_r, z_s, z_r,
    dz_s, dz_r, dx_s, dx_r, q1_s, q1_r, q2_s, q2_r, vz_s, vz_r, vx_s, vx_r,
    e1_s, e1_r, e2_s, e2_r, e3_s, e3_r, e4_s, e4_r,
):
    fs = lax.axis_index("fs")
    tp = lax.axis_index("tp")
    core = tp % 2
    other = 1 - core
    high_tp = tp // 2
    lo = fs % 2
    hi = fs // 2
    y_n = tp_n // 2
    h_n = fs_n // 2
    half_n = h_n // 2
    rows = factor.shape[0] // fs_n
    part = rows // 2
    rank_rows, width = mean.shape
    tokens, depth = x.shape
    sends = []

    def send(src, dst, ssem, rsem, device):
        copy = pltpu.make_async_remote_copy(
            src_ref=src, dst_ref=dst, send_sem=ssem, recv_sem=rsem,
            device_id=device, device_id_type=pl.DeviceIdType.MESH)
        copy.start()
        sends.append(copy)

    def arrive(dst, ssem, rsem, device):
        pltpu.make_async_remote_copy(
            src_ref=dst, dst_ref=dst, send_sem=ssem, recv_sem=rsem,
            device_id=device, device_id_type=pl.DeviceIdType.MESH).wait_recv()

    x_peer = (flip(fs, 1), tp)
    core_peer = (fs, flip(tp, 1))

    def z_peer(d):
        return (flip(hi, d) * 2 + lo, tp)

    def y_peer(d):
        return (fs, flip(high_tp, d) * 2 + core)

    def tp_peer(d):
        return (fs, flip(tp, d))

    def fs_peer(d):
        return (flip(fs, d), tp)

    def block(ref, index, size):
        return ref.at[pl.ds(pl.multiple_of(index * size, size), size)]

    def piece(index, which):
        return factor.at[pl.ds(pl.multiple_of(index * rows + which * part, part), part)]

    ins = [
        (factor_hbm, block(factor, fs, rows)), (dc_hbm, dc), (x_hbm, x), (c_hbm, c_in),
        (mean_hbm, mean), (second_hbm, second), (master_hbm, master),
        (dmean_hbm, dmean), (dsecond_hbm, dsecond), (dmaster_hbm, dmaster),
    ]
    loads = [pltpu.make_async_copy(s, d, in_sem.at[i]) for i, (s, d) in enumerate(ins)]
    for load in loads:
        load.start()

    barrier = pltpu.get_barrier_semaphore()
    for d in range(1, tp_n):
        pl.semaphore_signal(barrier, inc=1, device_id=tp_peer(d), device_id_type=pl.DeviceIdType.MESH)
    for d in range(1, fs_n):
        pl.semaphore_signal(barrier, inc=1, device_id=fs_peer(d), device_id_type=pl.DeviceIdType.MESH)
    pl.semaphore_wait(barrier, tp_n + fs_n - 2)

    loads[0].wait()
    mine = piece(fs, core)
    send(mine, mine, fx_s.at[0], fx_r.at[0], x_peer)
    for d in range(1, h_n):
        send(mine, mine, fz_s.at[d], fz_r.at[d], z_peer(d))

    def forward_z(d):
        ref = piece(flip(hi, d) * 2 + lo, core)
        arrive(ref, fz_s.at[d], fz_r.at[d], z_peer(d))
        send(ref, ref, fx_s.at[d], fx_r.at[d], x_peer)
        send(ref, ref, fc_s.at[0, d], fc_r.at[0, d], core_peer)

    def forward_x(d):
        ref = piece(flip(hi, d) * 2 + 1 - lo, core)
        arrive(ref, fx_s.at[d], fx_r.at[d], x_peer)
        send(ref, ref, fc_s.at[1, d], fc_r.at[1, d], core_peer)

    def arrive_core(d):
        for side in range(2):
            if side == 0 and d == 0:
                continue
            ref = piece(flip(hi, d) * 2 + (lo if side == 0 else 1 - lo), other)
            arrive(ref, fc_s.at[side, d], fc_r.at[side, d], core_peer)

    loads[1].wait()
    turned = dc[...]
    heads = turned.shape[0]
    unit = dpart.shape[2]
    loads[2].wait()
    for d in range(1, half_n):
        forward_z(d)
    forward_x(0)

    lane_tile = 2 * LANES
    for tile in range(depth // lane_tile):
        value = dot(turned, x[:, tile * lane_tile:(tile + 1) * lane_tile])
        for k in range(lane_tile // LANES):
            for h in range(0, heads, unit):
                b = ((tile * (lane_tile // LANES) + k) * heads + h) // unit
                dpart[b // fs_n, b % fs_n] = value[h:h + unit, k * LANES:(k + 1) * LANES]
    for d in range(1, tp_n):
        send(dpart.at[flip(tp, d)], dr_tp.at[d], e1_s.at[d], e1_r.at[d], tp_peer(d))

    for d in range(half_n, h_n):
        forward_z(d)
    for d in range(1, half_n):
        forward_x(d)
    for d in range(half_n):
        arrive_core(d)

    span = depth // 2
    near = hi // half_n
    tall = tokens // 6 if tokens % 6 == 0 else tokens

    def columns(which):
        return pl.ds(pl.multiple_of(which * span, span), span)

    near_cols, far_cols = columns(near), columns(1 - near)

    @pl.loop(0, tokens // tall)
    def _(i):
        r = pl.ds(pl.multiple_of(i * tall, tall), tall)
        mapped[r, :] = dot(x[r, near_cols], factor[near_cols, :])

    for d in range(half_n, h_n):
        forward_x(d)
    for d in range(half_n, h_n):
        arrive_core(d)

    @pl.loop(0, tokens // tall)
    def _(i):
        r = pl.ds(pl.multiple_of(i * tall, tall), tall)
        full = mapped[r, :] + dot(x[r, far_cols], factor[far_cols, :])
        full = jnp.transpose(full)
        top = full.astype(BF16)
        high[:, r] = top
        low[:, r] = (full - top.astype(F32)).astype(BF16)

    loads[3].wait()

    def chunk(c, y):
        cols = pl.ds(pl.multiple_of((y * 2 + c) * width, width), width)
        value = dot(high[...], c_in[:, cols]) + dot(low[...], c_in[:, cols])
        for f in range(fs_n):
            block_value = value[f * rank_rows:(f + 1) * rank_rows]
            h, xx = f // 2, f % 2
            if h < half_n:
                pa[c, y, xx, h] = block_value
            else:
                pb[c, xx, y, h - half_n] = block_value

    for y in range(y_n):
        chunk(other, y)
        send(pa.at[other, y], ra1.at[y], p1_s.at[0, y], p1_r.at[0, y], core_peer)
        send(pb.at[other, :, y], rb1.at[:, y], p1_s.at[1, y], p1_r.at[1, y], core_peer)

    for d in range(1, tp_n):
        arrive(dr_tp.at[d], e1_s.at[d], e1_r.at[d], tp_peer(d))
    total = dpart[tp]
    for d in range(1, tp_n):
        total = total + dr_tp[d]
    dmid[...] = total
    for d in range(1, fs_n):
        send(dmid.at[flip(fs, d)], dr_fs.at[d], e2_s.at[d], e2_r.at[d], fs_peer(d))

    for y in range(y_n):
        chunk(core, y)
    for y in range(y_n):
        arrive(ra1.at[y], p1_s.at[0, y], p1_r.at[0, y], core_peer)
        arrive(rb1.at[:, y], p1_s.at[1, y], p1_r.at[1, y], core_peer)
    pb[core] = pb[core] + rb1[...]
    send(pb.at[core, 1 - lo], rb2, b2_s, b2_r, x_peer)
    pa[core] = pa[core] + ra1[...]
    for d in range(1, y_n):
        send(pa.at[core, flip(high_tp, d)], ra2.at[d], a2_s.at[d], a2_r.at[d], y_peer(d))

    for d in range(1, fs_n):
        arrive(dr_fs.at[d], e2_s.at[d], e2_r.at[d], fs_peer(d))
    tile_sum = dmid[fs]
    for d in range(1, fs_n):
        tile_sum = tile_sum + dr_fs[d]
    dgrad[tp, fs] = tile_sum
    own_tile = dgrad.at[tp, fs]
    for d in range(1, fs_n):
        send(own_tile, own_tile, e3_s.at[d], e3_r.at[d], fs_peer(d))

    for d in range(1, y_n):
        arrive(ra2.at[d], a2_s.at[d], a2_r.at[d], y_peer(d))
    value = pa[core, high_tp]
    for d in range(1, y_n):
        value = value + ra2[d]
    pa[core, high_tp] = value
    send(pa.at[core, high_tp, 1 - lo], ra3, a3_s, a3_r, x_peer)
    arrive(rb2, b2_s, b2_r, x_peer)
    pb[core, lo] = pb[core, lo] + rb2[...]
    for d in range(1, y_n):
        send(pb.at[core, lo, flip(high_tp, d)], rb3.at[d], b3_s.at[d], b3_r.at[d], y_peer(d))

    arrive(ra3, a3_s, a3_r, x_peer)
    zed[0:half_n] = pa[core, high_tp, lo] + ra3[...]
    for d in range(1, y_n):
        arrive(rb3.at[d], b3_s.at[d], b3_r.at[d], y_peer(d))
    value = pb[core, lo, high_tp]
    for d in range(1, y_n):
        value = value + rb3[d]
    zed[half_n:h_n] = value
    for d in reversed(range(1, h_n)):
        send(zed.at[flip(hi, d)], rz.at[d], z_s.at[d], z_r.at[d], z_peer(d))

    for d in range(1, fs_n):
        ref = dgrad.at[tp, flip(fs, d)]
        arrive(ref, e3_s.at[d], e3_r.at[d], fs_peer(d))
    own_row = dgrad.at[tp]
    for d in range(1, tp_n):
        send(own_row, own_row, e4_s.at[d], e4_r.at[d], tp_peer(d))

    loads[4].wait()
    loads[5].wait()
    loads[6].wait()
    for d in range(1, h_n):
        arrive(rz.at[d], z_s.at[d], z_r.at[d], z_peer(d))
    projected = zed[hi]
    for d in range(1, h_n):
        projected = projected + rz[d]

    mean_new, second_new, own_direction = adam(mean[...], second[...], projected)
    own_dir = block(direction, fs, rank_rows)
    direction[pl.ds(pl.multiple_of(fs * rank_rows, rank_rows), rank_rows), :] = own_direction
    for d in reversed(range(1, h_n)):
        send(own_dir, own_dir, dz_s.at[d], dz_r.at[d], z_peer(d))
    send(own_dir, own_dir, dx_s.at[0], dx_r.at[0], x_peer)
    mean_v[...] = mean_new
    second_v[...] = second_new
    stores = []

    def store(src, dst):
        copy = pltpu.make_async_copy(src, dst, out_sem.at[len(stores)])
        copy.start()
        stores.append(copy)

    store(mean_v, mean_out)
    store(second_v, second_out)
    for d in range(1, h_n):
        ref = block(direction, flip(hi, d) * 2 + lo, rank_rows)
        arrive(ref, dz_s.at[d], dz_r.at[d], z_peer(d))
        send(ref, ref, dx_s.at[d], dx_r.at[d], x_peer)
    for d in range(h_n):
        ref = block(direction, flip(hi, d) * 2 + 1 - lo, rank_rows)
        arrive(ref, dx_s.at[d], dx_r.at[d], x_peer)

    whole = direction[...]
    whole_top = whole.astype(BF16)
    whole_low = (whole - whole_top.astype(F32)).astype(BF16)
    own_rows = pl.ds(pl.multiple_of(fs * rows, rows), rows)
    own_factor = factor[own_rows, :]
    raw = dot(own_factor, whole_top) + dot(own_factor, whole_low)
    squares[0] = jnp.sum(raw * raw, axis=0, keepdims=True)
    for d in range(1, tp_n):
        send(squares.at[0], sq_tp.at[d], q1_s.at[d], q1_r.at[d], tp_peer(d))
    step_v[...] = raw
    for d in range(1, tp_n):
        arrive(sq_tp.at[d], q1_s.at[d], q1_r.at[d], tp_peer(d))
    total = squares[0]
    for d in range(1, tp_n):
        total = total + sq_tp[d]
    squares[1] = total
    for d in range(1, fs_n):
        send(squares.at[1], sq_fs.at[d], q2_s.at[d], q2_r.at[d], fs_peer(d))
    for d in range(1, fs_n):
        arrive(sq_fs.at[d], q2_s.at[d], q2_r.at[d], fs_peer(d))
    for d in range(1, fs_n):
        total = total + sq_fs[d]
    scale = lax.rsqrt(jnp.sum(total, axis=1, keepdims=True) / (depth * width * tp_n) + RMS_EPS)
    value_step = step_v[...] * scale
    value_new = master[...] - LEARN_RATE * value_step
    copy_v[own_rows, :] = value_new.astype(BF16)
    own_copy = block(copy_v, fs, rows)
    send(own_copy, own_copy, vx_s.at[0], vx_r.at[0], x_peer)
    for d in range(1, h_n):
        send(own_copy, own_copy, vz_s.at[d], vz_r.at[d], z_peer(d))
    step_v[...] = value_step
    new_v[...] = value_new
    store(step_v, step_out)
    store(new_v, new_out)

    def forward_copy(d):
        index = flip(hi, d) * 2 + lo
        ref = block(copy_v, index, rows)
        arrive(ref, vz_s.at[d], vz_r.at[d], z_peer(d))
        send(ref, ref, vx_s.at[d], vx_r.at[d], x_peer)

    for d in range(1, tp_n):
        ref = dgrad.at[flip(tp, d)]
        arrive(ref, e4_s.at[d], e4_r.at[d], tp_peer(d))
    for load in loads[7:]:
        load.wait()
    per_lane = heads // unit
    forward_at = {}
    blocks = depth // LANES
    for d in range(1, h_n):
        forward_at.setdefault(min(blocks - 1, d * blocks // h_n), []).append(d)
    for lane in range(blocks):
        tiles = []
        for k in range(per_lane):
            b = lane * per_lane + k
            tiles.append(dgrad[b // fs_n, b % fs_n])
        grad = jnp.concatenate(tiles, axis=0)
        r = slice(lane * LANES, (lane + 1) * LANES)
        unused_mean, unused_second, dstep = adam(dmean[:, r], dsecond[:, r], grad)
        dstep_v[:, r] = dstep
        dcopy_v[:, r] = (dmaster[:, r] - LEARN_RATE * dstep).astype(BF16)
        for d in forward_at.get(lane, ()):
            forward_copy(d)
    store(dstep_v, dstep_out)
    store(dcopy_v, dcopy_out)
    for d in range(h_n):
        ref = block(copy_v, flip(hi, d) * 2 + 1 - lo, rows)
        arrive(ref, vx_s.at[d], vx_r.at[d], x_peer)
    store(copy_v, copy_out)
    for copy in sends:
        copy.wait_send()
    for copy in stores:
        copy.wait()


def local(fs_n, tp_n, *args):
    x, c_in, dc, master, factor, mean, second, dmaster, dmean, dsecond = args
    rows, rank = factor.shape
    rank_rows, width = mean.shape
    tokens, depth = x.shape
    dc, dmaster, dmean, dsecond = dc.T, dmaster.T, dmean.T, dsecond.T
    args = (x, c_in, dc, master, factor, mean, second, dmaster, dmean, dsecond)
    heads = dc.shape[0]
    h_n, y_n = fs_n // 2, tp_n // 2
    half_n = h_n // 2
    unit = heads * (depth // LANES) // (fs_n * tp_n)
    v = pltpu.VMEM
    shape = jax.ShapeDtypeStruct
    dma = lambda *n: pltpu.SemaphoreType.DMA(n)
    pair = lambda *n: [dma(*n), dma(*n)]
    single = [pltpu.SemaphoreType.DMA, pltpu.SemaphoreType.DMA]
    scratch = [
        v(x.shape, BF16), v(c_in.shape, BF16), v(dc.shape, BF16), v(master.shape, F32),
        v((depth, rank), BF16), v(mean.shape, F32), v(second.shape, F32),
        v(dmaster.shape, F32), v(dmean.shape, F32), v(dsecond.shape, F32),
        v((tokens, rank), F32), v((rank, tokens), BF16), v((rank, tokens), BF16),
        v((2, y_n, 2, half_n, rank_rows, width), F32),
        v((2, 2, y_n, half_n, rank_rows, width), F32),
        v((y_n, 2, half_n, rank_rows, width), F32),
        v((2, y_n, half_n, rank_rows, width), F32),
        v((y_n, 2, half_n, rank_rows, width), F32),
        v((y_n, half_n, rank_rows, width), F32),
        v((half_n, rank_rows, width), F32),
        v((y_n, half_n, rank_rows, width), F32),
        v((h_n, rank_rows, width), F32), v((h_n, rank_rows, width), F32),
        v((rank, width), F32), v((2, 1, width), F32),
        v((tp_n, 1, width), F32), v((fs_n, 1, width), F32),
        v(master.shape, F32), v(master.shape, F32), v((depth, width), BF16),
        v(mean.shape, F32), v(mean.shape, F32),
        v((tp_n, fs_n, unit, LANES), F32), v((tp_n, fs_n, unit, LANES), F32),
        v((fs_n, unit, LANES), F32), v((fs_n, unit, LANES), F32),
        v((tp_n, fs_n, unit, LANES), F32), v(dmean.shape, F32), v(dmean.shape, BF16),
        dma(10), dma(7),
        *pair(h_n), *pair(h_n), *pair(2, h_n),
        *pair(2, y_n), *pair(y_n), *single, *single, *pair(y_n), *pair(h_n),
        *pair(h_n), *pair(h_n), *pair(tp_n), *pair(fs_n), *pair(h_n), *pair(h_n),
        *pair(tp_n), *pair(fs_n), *pair(fs_n), *pair(tp_n),
    ]
    outs = pl.pallas_call(
        functools.partial(kernel, fs_n, tp_n),
        out_shape=(
            shape(master.shape, F32), shape(master.shape, F32), shape((depth, width), BF16),
            shape(mean.shape, F32), shape(mean.shape, F32),
            shape(dmean.shape, F32), shape(dmean.shape, BF16),
        ),
        in_specs=[pl.BlockSpec(memory_space=pl.ANY)] * 10,
        out_specs=[pl.BlockSpec(memory_space=pl.ANY)] * 7,
        scratch_shapes=scratch,
        compiler_params=pltpu.CompilerParams(
            collective_id=0, has_side_effects=True, vmem_limit_bytes=56 * 1024 * 1024),
    )(*args)
    return (*outs[:5], outs[5].T, outs[6].T)


def solution(mesh):
    split = P(("fs", "tp"), None)
    in_specs = (split, split, split, P("fs", "tp"), P("fs", None), P("fs", "tp"), P("fs", "tp"), P(), P(), P())
    out_specs = (P("fs", "tp"), P("fs", "tp"), P(None, "tp"), P("fs", "tp"), P("fs", "tp"), P(), P())
    body = functools.partial(local, mesh.shape["fs"], mesh.shape["tp"])
    return jax.shard_map(body, mesh=mesh, in_specs=in_specs, out_specs=out_specs, check_vma=False)
```

profile of v0, /device:TPU:0, one launch (start us, length us, event | category | flops | bytes accessed | tf_op | source)
XLA Modules:
  0.0 81.3 jit_solution(4028598055405612500)
XLA Ops:
  0.6 69.3 %shard_map.153 = (f32[256,256]{1,0:T(8,128)}, f32[256,256]{1,0:T(8,128)}, bf16[2048,256]{1,0:T(8,128)(2,1)}, f32[32,256]{1,0:T(8,128)}, f32[32,256]{1,0:T(8,128)...) custom-call(bf16[1536,2048]{1,0:T(8,128)(2,1)} %x_hbm.1, bf16[1536,1024]{1,0:T(8,128)(2,1)} %c_hbm.1, ...), custom_call_target="tpu_custom_call" | custom-call | tf_op jit(solution)/shard_map/pallas_call | solution.py:428
  69.9 1.7 %copy.24 = f32[256,256]{1,0:T(8,128)} copy(f32[256,256]{1,0:T(8,128)} %get-tuple-element.28) | data formatting | bytes 524288
  71.6 1.7 %copy.25 = f32[256,256]{1,0:T(8,128)} copy(f32[256,256]{1,0:T(8,128)} %get-tuple-element.29) | data formatting | bytes 524288
  73.3 2.3 %copy.26 = bf16[2048,256]{1,0:T(8,128)(2,1)} copy(bf16[2048,256]{1,0:T(8,128)(2,1)} %get-tuple-element.30) | data formatting | bytes 2097152
  75.5 1.4 %copy.27 = f32[32,256]{1,0:T(8,128)} copy(f32[32,256]{1,0:T(8,128)} %get-tuple-element.31) | data formatting | bytes 65536
  76.9 1.4 %copy.28 = f32[32,256]{1,0:T(8,128)} copy(f32[32,256]{1,0:T(8,128)} %get-tuple-element.32) | data formatting | bytes 65536
  78.3 1.6 %copy.29 = f32[2048,16]{0,1:T(8,128)} copy(f32[2048,16]{0,1:T(8,128)} %bitcast.9) | data formatting | bytes 262144
  79.8 1.5 %copy.30 = bf16[2048,16]{0,1:T(8,128)(2,1)} copy(bf16[2048,16]{0,1:T(8,128)(2,1)} %bitcast.10) | data formatting | bytes 131072
where the time goes:
time: 81.7 us; the launch traced here: 81.3 us
  Pallas kernels  69.3 us (85%)
  local copies, waits for them, and re-layouts  11.4 us (14%)
    pallas_call x1, Pallas kernels, local(): pl.pallas_call(functools.partial(kernel, fs_n, tp_n), out_shape=(shape(ma...  69.3 us
    unnamed x7, local copies, waits for them, and re-layouts  11.4 us

commit v1 on v0

--- a/solution.py
+++ b/solution.py
@@ -41,15 +41,15 @@
     fs_n, tp_n,
     x_hbm, c_hbm, dc_hbm, master_hbm, factor_hbm, mean_hbm, second_hbm,
     dmaster_hbm, dmean_hbm, dsecond_hbm,
-    step_out, new_out, copy_out, mean_out, second_out, dstep_out, dcopy_out,
+    step_v, new_v, copy_v, mean_v, second_v, dstep_v, dcopy_v,
     x, c_in, dc, master, factor, mean, second, dmaster, dmean, dsecond,
     mapped, high, low, pa, pb, ra1, rb1, ra2, rb2, ra3, rb3, zed, rz,
-    direction, squares, sq_tp, sq_fs, step_v, new_v, copy_v, mean_v, second_v,
-    dpart, dr_tp, dmid, dr_fs, dgrad, dstep_v, dcopy_v,
-    in_sem, out_sem,
+    direction, squares, sq_tp,
+    dpart, dr_tp, dmid, dr_fs, dgrad,
+    in_sem,
     fz_s, fz_r, fx_s, fx_r, fc_s, fc_r,
     p1_s, p1_r, a2_s, a2_r, b2_s, b2_r, a3_s, a3_r, b3_s, b3_r, z_s, z_r,
-    dz_s, dz_r, dx_s, dx_r, q1_s, q1_r, q2_s, q2_r, vz_s, vz_r, vx_s, vx_r,
+    dz_s, dz_r, dx_s, dx_r, q1_s, q1_r, vz_s, vz_r, vx_s, vx_r,
     e1_s, e1_r, e2_s, e2_r, e3_s, e3_r, e4_s, e4_r,
 ):
     fs = lax.axis_index("fs")
@@ -290,15 +290,6 @@
     send(own_dir, own_dir, dx_s.at[0], dx_r.at[0], x_peer)
     mean_v[...] = mean_new
     second_v[...] = second_new
-    stores = []
-
-    def store(src, dst):
-        copy = pltpu.make_async_copy(src, dst, out_sem.at[len(stores)])
-        copy.start()
-        stores.append(copy)
-
-    store(mean_v, mean_out)
-    store(second_v, second_out)
     for d in range(1, h_n):
         ref = block(direction, flip(hi, d) * 2 + lo, rank_rows)
         arrive(ref, dz_s.at[d], dz_r.at[d], z_peer(d))
@@ -311,25 +302,26 @@
     whole_top = whole.astype(BF16)
     whole_low = (whole - whole_top.astype(F32)).astype(BF16)
     own_rows = pl.ds(pl.multiple_of(fs * rows, rows), rows)
-    own_factor = factor[own_rows, :]
-    raw = dot(own_factor, whole_top) + dot(own_factor, whole_low)
-    squares[0] = jnp.sum(raw * raw, axis=0, keepdims=True)
-    for d in range(1, tp_n):
-        send(squares.at[0], sq_tp.at[d], q1_s.at[d], q1_r.at[d], tp_peer(d))
-    step_v[...] = raw
+
+    def update(r):
+        return dot(factor[r, :], whole_top) + dot(factor[r, :], whole_low)
+
+    squares[...] = jnp.zeros_like(squares)
+
+    @pl.loop(0, fs_n)
+    def _(i):
+        raw = update(pl.ds(pl.multiple_of(i * rows, rows), rows))
+        squares[...] += jnp.sum((raw * raw).reshape(rows // 8, 8, width), axis=0)
+
+    for d in range(1, tp_n):
+        send(squares, sq_tp.at[d], q1_s.at[d], q1_r.at[d], tp_peer(d))
+    step_v[...] = update(own_rows)
+    total = squares[...]
     for d in range(1, tp_n):
         arrive(sq_tp.at[d], q1_s.at[d], q1_r.at[d], tp_peer(d))
-    total = squares[0]
-    for d in range(1, tp_n):
         total = total + sq_tp[d]
-    squares[1] = total
-    for d in range(1, fs_n):
-        send(squares.at[1], sq_fs.at[d], q2_s.at[d], q2_r.at[d], fs_peer(d))
-    for d in range(1, fs_n):
-        arrive(sq_fs.at[d], q2_s.at[d], q2_r.at[d], fs_peer(d))
-    for d in range(1, fs_n):
-        total = total + sq_fs[d]
-    scale = lax.rsqrt(jnp.sum(total, axis=1, keepdims=True) / (depth * width * tp_n) + RMS_EPS)
+    total = jnp.sum(jnp.sum(total, axis=0, keepdims=True), axis=1, keepdims=True)
+    scale = lax.rsqrt(total / (depth * width * tp_n) + RMS_EPS)
     value_step = step_v[...] * scale
     value_new = master[...] - LEARN_RATE * value_step
     copy_v[own_rows, :] = value_new.astype(BF16)
@@ -339,8 +331,6 @@
         send(own_copy, own_copy, vz_s.at[d], vz_r.at[d], z_peer(d))
     step_v[...] = value_step
     new_v[...] = value_new
-    store(step_v, step_out)
-    store(new_v, new_out)
 
     def forward_copy(d):
         index = flip(hi, d) * 2 + lo
@@ -370,15 +360,19 @@
         dcopy_v[:, r] = (dmaster[:, r] - LEARN_RATE * dstep).astype(BF16)
         for d in forward_at.get(lane, ()):
             forward_copy(d)
-    store(dstep_v, dstep_out)
-    store(dcopy_v, dcopy_out)
     for d in range(h_n):
         ref = block(copy_v, flip(hi, d) * 2 + 1 - lo, rows)
         arrive(ref, vx_s.at[d], vx_r.at[d], x_peer)
-    store(copy_v, copy_out)
     for copy in sends:
         copy.wait_send()
-    for copy in stores:
+
+
+def write_out(*refs):
+    held, outs, sem = refs[:7], refs[7:14], refs[14]
+    copies = [pltpu.make_async_copy(h, o, sem.at[i]) for i, (h, o) in enumerate(zip(held, outs))]
+    for copy in copies:
+        copy.start()
+    for copy in copies:
         copy.wait()
 
 
@@ -412,32 +406,38 @@
         v((half_n, rank_rows, width), F32),
         v((y_n, half_n, rank_rows, width), F32),
         v((h_n, rank_rows, width), F32), v((h_n, rank_rows, width), F32),
-        v((rank, width), F32), v((2, 1, width), F32),
-        v((tp_n, 1, width), F32), v((fs_n, 1, width), F32),
-        v(master.shape, F32), v(master.shape, F32), v((depth, width), BF16),
-        v(mean.shape, F32), v(mean.shape, F32),
+        v((rank, width), F32), v((8, width), F32), v((tp_n, 8, width), F32),
         v((tp_n, fs_n, unit, LANES), F32), v((tp_n, fs_n, unit, LANES), F32),
         v((fs_n, unit, LANES), F32), v((fs_n, unit, LANES), F32),
-        v((tp_n, fs_n, unit, LANES), F32), v(dmean.shape, F32), v(dmean.shape, BF16),
-        dma(10), dma(7),
+        v((tp_n, fs_n, unit, LANES), F32),
+        dma(10),
         *pair(h_n), *pair(h_n), *pair(2, h_n),
         *pair(2, y_n), *pair(y_n), *single, *single, *pair(y_n), *pair(h_n),
-        *pair(h_n), *pair(h_n), *pair(tp_n), *pair(fs_n), *pair(h_n), *pair(h_n),
+        *pair(h_n), *pair(h_n), *pair(tp_n), *pair(h_n), *pair(h_n),
         *pair(tp_n), *pair(fs_n), *pair(fs_n), *pair(tp_n),
     ]
-    outs = pl.pallas_call(
+    results = (
+        (master.shape, F32), (master.shape, F32), ((depth, width), BF16),
+        (mean.shape, F32), (mean.shape, F32), (dmean.shape, F32), (dmean.shape, BF16),
+    )
+    held = pl.pallas_call(
         functools.partial(kernel, fs_n, tp_n),
-        out_shape=(
-            shape(master.shape, F32), shape(master.shape, F32), shape((depth, width), BF16),
-            shape(mean.shape, F32), shape(mean.shape, F32),
-            shape(dmean.shape, F32), shape(dmean.shape, BF16),
-        ),
+        out_shape=tuple(v(*r) for r in results),
         in_specs=[pl.BlockSpec(memory_space=pl.ANY)] * 10,
-        out_specs=[pl.BlockSpec(memory_space=pl.ANY)] * 7,
+        out_specs=[pl.BlockSpec(memory_space=v)] * 7,
         scratch_shapes=scratch,
         compiler_params=pltpu.CompilerParams(
-            collective_id=0, has_side_effects=True, vmem_limit_bytes=56 * 1024 * 1024),
-    )(*args)
+            collective_id=0, has_side_effects=True, vmem_limit_bytes=48 * 1024 * 1024),
+    )(*[pltpu.with_memory_space_constraint(a, pltpu.HBM) for a in args])
+    held = [pltpu.with_memory_space_constraint(h, v) for h in held]
+    outs = pl.pallas_call(
+        write_out,
+        out_shape=tuple(shape(*r) for r in results),
+        in_specs=[pl.BlockSpec(memory_space=v)] * 7,
+        out_specs=[pl.BlockSpec(memory_space=pl.ANY)] * 7,
+        scratch_shapes=[dma(7)],
+        compiler_params=pltpu.CompilerParams(vmem_limit_bytes=1024 * 1024),
+    )(*held)
     return (*outs[:5], outs[5].T, outs[6].T)
 
 

time: 81.7 us -> 68.1 us (0.83)
  local copies, waits for them, and re-layouts: 11.4 us -> 0 us
  Pallas kernels: 69.3 us -> 67.3 us
    unnamed x7 -> x0, local copies, waits for them, and re-layouts: 11.4 us -> none
    pallas_call x1 -> x2, Pallas kernels: 69.3 us -> 67.3 us  [the longest x1 66 us: local(): pl.pallas_call(functools.partial(kernel, fs_n, tp_n), out_shape=tuple((v(...]
where the time goes in v1:
time: 68.1 us; the launch traced here: 68 us
  Pallas kernels  67.3 us (99%)
    pallas_call x1, Pallas kernels, local(): pl.pallas_call(functools.partial(kernel, fs_n, tp_n), out_shape=tuple((v(...  66 us

profile of v1, /device:TPU:0, one launch (start us, length us, event | category | flops | bytes accessed | tf_op | source)
XLA Modules:
  0.0 68.0 jit_solution(15590773863756381113)
XLA Ops:
  0.6 66.0 %shard_map.153 = (f32[256,256]{1,0:T(8,128)S(1)}, f32[256,256]{1,0:T(8,128)S(1)}, bf16[2048,256]{1,0:T(8,128)(2,1)S(1)}, f32[32,256]{1,0:T(8,128)S(1)}, f32[32,2...) custom-call(bf16[1536,2048]{1,0:T(8,128)(2,1)} %x_hbm.1, bf16[1536,1024]{1,0:T(8,128)(2,1)} %c_hbm.1, ...), custom_call_target="tpu_custom_call" | custom-call | tf_op jit(solution)/shard_map/pallas_call | solution.py:423
  66.7 1.3 %shard_map.154 = (f32[256,256]{1,0:T(8,128)}, f32[256,256]{1,0:T(8,128)}, bf16[2048,256]{1,0:T(8,128)(2,1)}, f32[32,256]{1,0:T(8,128)}, f32[32,256]{1,0:T(8,128)...) custom-call(f32[256,256]{1,0:T(8,128)S(1)} %get-tuple-element.21.refs_0_, f32[256,256]{1,0:T(8,128)S(1)} %get-tuple-element.22.refs_1_, ...), custom_call_target="tpu_custom_call" | custom-call | tf_op jit(solution)/shard_map/pallas_call | solution.py:433
